TPU v7x, 32 devices: a whole 2x2x4 slice. The times are simulated.
32 devices in a mesh: sp: 16 (over z, y, x), tp: 2 (over core).
Axes of the slice: x: 2, y: 2, z: 4, core: 2. Of those that a mesh axis runs over, the one named last changes fastest.
Arguments:
- stream: bfloat16 [1024, 8192], P('tp', 'sp'), may hold values from -6 to 6
- norm_gain: float32 [2, 1024], replicated, may hold values from 0.1 to 1.9
- w_value: bfloat16 [2, 512, 1024], P(None, 'tp'), may hold values from -0.1875 to 0.1875
- w_gate: bfloat16 [2, 512, 1024], P(None, 'tp'), may hold values from -0.1875 to 0.1875
- conv_taps: bfloat16 [2, 512, 255], P(None, 'tp'), may hold values from -0.375 to 0.375
- group_gain: float32 [2, 512], P(None, 'tp'), may hold values from 0.1 to 1.9
- group_shift: float32 [2, 512], P(None, 'tp'), may hold values from -3 to 3
- w_out: bfloat16 [2, 1024, 512], P(None, 'tp'), may hold values from -0.25 to 0.25
Outputs:
- result: bfloat16 [1024, 8192], P('tp', 'sp')
All inputs are finite; a program needn't handle non-finite values.
Results may differ from a plain program's by a relative error of at most 0.014.
Values may be sent and summed in bfloat16 or wider, within the bound.
A program may use at most 64 MiB of HBM per device.

v0:
```python
import jax
import jax.numpy as jnp
from jax import lax
from jax.sharding import PartitionSpec as P

GROUP_DIM = 128


RMS_EPS = 1e-06
LN_EPS = 1e-05


def with_halo(cells, sides, width):
    for axis, dim in sides:
        count = lax.axis_size(axis)
        ends = count - 1
        head = lax.slice_in_dim(cells, 0, width, axis=dim)
        tail = lax.slice_in_dim(cells, cells.shape[dim] - width, cells.shape[dim], axis=dim)
        cells = jnp.concatenate(
            [
                lax.ppermute(tail, axis, [(i, (i + 1) % count) for i in range(ends)]),
                cells,
                lax.ppermute(head, axis, [((i + 1) % count, i) for i in range(ends)]),
            ],
            axis=dim,
        )
    return cells


def make_gated(whole, gain, value_weight, gate_weight):
    widened = whole.astype(jnp.float32)
    inverse_rms = lax.rsqrt(jnp.mean(widened * widened, axis=0, keepdims=True) + RMS_EPS)
    normed = (widened * inverse_rms * gain[:, None]).astype(jnp.bfloat16)
    projected = jnp.dot(value_weight, normed, preferred_element_type=jnp.float32).astype(
        jnp.bfloat16
    )
    gate_proj = jnp.dot(gate_weight, normed, preferred_element_type=jnp.float32).astype(
        jnp.bfloat16
    )
    return (projected.astype(jnp.float32) * jax.nn.sigmoid(gate_proj.astype(jnp.float32))).astype(
        jnp.bfloat16
    )


def filter_norm(padded, taps, ggain, gshift):
    channels = taps.shape[0]
    filtered = lax.conv_general_dilated(
        padded[None],
        taps[:, None, :],
        (1,),
        [(0, 0)],
        dimension_numbers=("NCW", "OIW", "NCW"),
        feature_group_count=channels,
        preferred_element_type=jnp.float32,
    )[0]
    tokens_here = filtered.shape[1]
    grouped = filtered.reshape(channels // GROUP_DIM, GROUP_DIM, tokens_here)
    group_mean = jnp.mean(grouped, axis=1, keepdims=True)
    centred = grouped - group_mean
    scaled = centred * lax.rsqrt(jnp.mean(centred * centred, axis=1, keepdims=True) + LN_EPS)
    scaled = scaled.reshape(channels, tokens_here) * ggain[:, None] + gshift[:, None]
    return jax.nn.silu(scaled).astype(jnp.bfloat16)


def body(stream, norm_gain, w_value, w_gate, conv_taps, group_gain, group_shift, w_out):
    rim_width = (conv_taps.shape[2] - 1) // 2
    layers = w_value.shape[0]
    local = lax.all_to_all(stream, "tp", split_axis=1, concat_axis=0, tiled=True)
    full_value, full_gate, full_taps, full_out = (
        lax.all_gather(w_value, "tp", axis=1, tiled=True),
        lax.all_gather(w_gate, "tp", axis=1, tiled=True),
        lax.all_gather(conv_taps, "tp", axis=1, tiled=True),
        lax.all_gather(w_out, "tp", axis=1, tiled=True),
    )
    full_ggain, full_gshift = (
        lax.all_gather(group_gain, "tp", axis=1, tiled=True),
        lax.all_gather(group_shift, "tp", axis=1, tiled=True),
    )
    for layer_index in range(layers):
        gated = make_gated(
            local, norm_gain[layer_index], full_value[layer_index], full_gate[layer_index]
        )
        padded = with_halo(gated, ((("sp", "tp"), 1),), rim_width)
        activated = filter_norm(
            padded, full_taps[layer_index], full_ggain[layer_index], full_gshift[layer_index]
        )
        branch = jnp.dot(full_out[layer_index], activated, preferred_element_type=jnp.float32)
        local = (local.astype(jnp.float32) + branch).astype(jnp.bfloat16)
    return lax.all_to_all(local, "tp", split_axis=0, concat_axis=1, tiled=True)


def solution(mesh):
    placed = (
        P("tp", "sp"),
        P(),
        P(None, "tp", None),
        P(None, "tp", None),
        P(None, "tp", None),
        P(None, "tp"),
        P(None, "tp"),
        P(None, "tp", None),
    )
    return jax.shard_map(body, mesh=mesh, in_specs=placed, out_specs=P("tp", "sp"), check_vma=False)
```

profile of v0, /device:TPU:0, one launch (start us, length us, event | category | flops | bytes accessed | tf_op | source)
XLA Modules:
  0.0 101.9 jit_solution(15479149076552450457)
XLA Ops:
  6.5 0.7 all-gather.4.cloned.1.call-update
  7.3 0.0 all-gather.6.cloned.1.call-start
  7.3 0.7 all-gather.6.cloned.1.call-update
  8.0 1.0 copy.38
  9.0 3.5 %all-to-all-start = ((bf16[512,2,256]{0,2,1:T(8,128)(2,1)}), bf16[512,2,256]{0,2,1:T(8,128)(2,1)S(1)}, u32[]{:S(2)}, u32[]{:S(2)}) async-start(bf16[512,2,256]{0,2,1:T(8,128)(2,1)} %bitcast), calls=%async_computation | async-start | bytes 1048576 | tf_op jit(solution)/shard_map/all_to_all | solution.py:68
  12.5 0.0 copy-start.2
  12.5 0.0 all-gather.8.cloned.1.call-start
  12.6 0.7 all-gather.8.cloned.1.call-update
  13.3 1.0 all-to-all-done
  14.2 0.2 copy.39
  14.5 0.2 multiply_reduce_fusion
  14.6 0.1 convert_element_type.131
  14.8 0.2 copy.41
  15.0 2.2 %all_gather.20 = bf16[2,512,255]{2,1,0:T(8,128)(2,1)S(1)} all-gather(bf16[2,256,255]{2,1,0:T(8,128)(2,1)S(1)} %copy.41), channel_id=1, replica_groups=mesh['sp'=16,'tp'=2] {'tp'}, dimensions={1}, use_global_device_ids=true | all-gather | bytes 783360 | tf_op jit(solution)/shard_map/all_gather | solution.py:72
  17.2 0.6 copy.43
  17.8 1.8 %all_gather.21 = f32[2,512]{1,0:T(2,128)S(1)} all-gather(f32[2,256]{1,0:T(2,128)S(1)} %copy-done.3), channel_id=1, replica_groups=mesh['sp'=16,'tp'=2] {'tp'}, dimensions={1}, use_global_device_ids=true | all-gather | bytes 6144 | tf_op jit(solution)/shard_map/all_gather | solution.py:76
  19.6 1.9 %all_gather.22 = f32[2,512]{1,0:T(2,128)S(1)} all-gather(f32[2,256]{1,0:T(2,128)S(1)} %copy-done.4), channel_id=1, replica_groups=mesh['sp'=16,'tp'=2] {'tp'}, dimensions={1}, use_global_device_ids=true | all-gather | bytes 6144 | tf_op jit(solution)/shard_map/all_gather | solution.py:77
  21.5 0.3 copy.48
  21.8 0.2 fusion.24
  22.0 0.2 all-gather.4.cloned.1.call-done
  22.2 1.7 %fusion.18 = f32[256,512]{1,0:T(8,128)S(1)} fusion(bf16[1024,256]{1,0:T(8,128)(2,1)S(1)} %bitcast.94, bf16[2,512,1024]{2,1,0:T(8,128)(2,1)} %all-gather.4.cloned.1.call-done), kind=kOutput, calls=%fused_computation.27 | convolution fusion | flops 268697600 | bytes 2097152 | tf_op jit(solution)/shard_map/dot_general | solution.py:34
  23.9 11.6 %all-gather.6.cloned.1.call-done = bf16[2,512,1024]{2,1,0:T(8,128)(2,1)} async-done(((bf16[2,256,1024]{2,1,0:T(8,128)(2,1)}), bf16[2,512,1024]{2,1,0:T(8,128)(2,1)}) %all-gather.6.cloned.1.call-update) | async-done | bytes 2097168 | tf_op jit(solution)/shard_map/all_gather | solution.py:71
  35.5 1.8 %fusion.19 = bf16[512,256]{0,1:T(8,128)(2,1)S(1)} fusion(f32[256,512]{1,0:T(8,128)S(1)} %fusion.18, bf16[1024,256]{1,0:T(8,128)(2,1)S(1)} %bitcast.95, bf16[2,512,1024]{2,1,0:T(8,128)(2,1)} %all-gather.6.cloned.1.call-done), kind=kOutput, calls=%fused_computation.28 | convolution fusion | flops 269352960 | bytes 2359296 | tf_op jit(solution)/shard_map/dot_general | solution.py:37
  37.4 2.1 %collective-permute-start = (bf16[512,127]{0,1:T(8,128)(2,1)S(1)}, bf16[512,127]{0,1:T(8,128)(2,1)S(1)}, u32[]{:S(2)}, u32[]{:S(2)}) collective-permute-start(bf16[512,127]{0,1:T(8,128)(2,1)S(1)} %get-tuple-element.9), channel_id=1, source_target_pairs={{0,1},{1,2},{2,3},{3,4},{4,5},{5,6},{6,7},{7,8},{8,9},{9,10},{10,1... | collective-permute-start | bytes 390152 | tf_op jit(solution)/shard_map/ppermute | solution.py:21
  39.5 1.3 %collective-permute-start.1 = (bf16[512,127]{0,1:T(8,128)(2,1)S(1)}, bf16[512,127]{0,1:T(8,128)(2,1)S(1)}, u32[]{:S(2)}, u32[]{:S(2)}) collective-permute-start(bf16[512,127]{0,1:T(8,128)(2,1)S(1)} %get-tuple-element.10), channel_id=1, source_target_pairs={{1,0},{2,1},{3,2},{4,3},{5,4},{6,5},{7,6},{8,7},{9,8},{10,9},{11,1... | collective-permute-start | bytes 390152 | tf_op jit(solution)/shard_map/ppermute | solution.py:23
  40.8 3.1 %collective-permute-done.1 = bf16[512,127]{0,1:T(8,128)(2,1)S(1)} collective-permute-done((bf16[512,127]{0,1:T(8,128)(2,1)S(1)}, bf16[512,127]{0,1:T(8,128)(2,1)S(1)}, u32[]{:S(2)}, u32[]{:S(2)}) %collective-permute-start.1) | collective-permute-done | bytes 130080 | tf_op jit(solution)/shard_map/ppermute | solution.py:23
  43.9 0.1 maximum_bitcast_fusion
  44.0 12.8 %fusion.27 = f32[1,512,256]{1,0,2:T(1,128)S(1)} fusion(bf16[512,1,255]{0,1,2:T(2,128)(2,1)S(1)} %copy.43, bf16[1,512,510]{1,2,0:T(8,128)(2,1)S(1)} %maximum_bitcast_fusion), kind=kOutput, calls=%fused_computation.44 | convolution fusion | flops 66846720 | bytes 1307648 | tf_op jit(solution)/shard_map/conv_general_dilated | solution.py:47
  56.8 0.3 reduce_sum.55
  57.2 0.6 multiply_reduce_fusion.2
  57.9 0.8 fusion.29
  58.6 0.0 all-gather.8.cloned.1.call-done
  58.7 1.9 %fusion.21 = (f32[256]{0:T(256)S(1)}, bf16[1024,256]{0,1:T(8,128)(2,1)S(1)}) fusion(f32[1024,256]{0,1:T(8,128)S(1)} %copy.48, bf16[2,1024,512]{2,1,0:T(8,128)(2,1)} %all-gather.8.cloned.1.call-done, bf16[32,8,4,128]{3,2,1,0:T(4,128)(2,1)S(1)} %bitcast.97), kind=kOutput, calls=%fused_computation.30 | convolution fusion | flops 269745920 | bytes 2884608 | tf_op jit(solution)/shard_map/dot_general | solution.py:87
  60.6 0.5 fusion.10
  61.1 1.1 %copy-done.7 = bf16[2,512,1024]{2,1,0:T(8,128)(2,1)S(1)} copy-done((bf16[2,512,1024]{2,1,0:T(8,128)(2,1)S(1)}, bf16[2,512,1024]{2,1,0:T(8,128)(2,1)}, u32[]{:S(2)}) %copy-start.7) | copy-done | bytes 2097176
  62.2 0.6 fusion.20
  62.8 5.5 %collective-permute-start.2 = (bf16[512,127]{0,1:T(8,128)(2,1)S(1)}, bf16[512,127]{0,1:T(8,128)(2,1)S(1)}, u32[]{:S(2)}, u32[]{:S(2)}) collective-permute-start(bf16[512,127]{0,1:T(8,128)(2,1)S(1)} %get-tuple-element.7), channel_id=1, source_target_pairs={{0,1},{1,2},{2,3},{3,4},{4,5},{5,6},{6,7},{7,8},{8,9},{9,10},{10,1... | collective-permute-start | bytes 390152 | tf_op jit(solution)/shard_map/ppermute | solution.py:21
  68.3 1.5 %collective-permute-start.3 = (bf16[512,127]{0,1:T(8,128)(2,1)S(1)}, bf16[512,127]{0,1:T(8,128)(2,1)S(1)}, u32[]{:S(2)}, u32[]{:S(2)}) collective-permute-start(bf16[512,127]{0,1:T(8,128)(2,1)S(1)} %get-tuple-element.8), channel_id=1, source_target_pairs={{1,0},{2,1},{3,2},{4,3},{5,4},{6,5},{7,6},{8,7},{9,8},{10,9},{11,1... | collective-permute-start | bytes 390152 | tf_op jit(solution)/shard_map/ppermute | solution.py:23
  69.8 0.6 copy.45
  70.3 1.2 %collective-permute-done.3 = bf16[512,127]{0,1:T(8,128)(2,1)S(1)} collective-permute-done((bf16[512,127]{0,1:T(8,128)(2,1)S(1)}, bf16[512,127]{0,1:T(8,128)(2,1)S(1)}, u32[]{:S(2)}, u32[]{:S(2)}) %collective-permute-start.3) | collective-permute-done | bytes 130080 | tf_op jit(solution)/shard_map/ppermute | solution.py:23
  71.5 0.1 maximum_bitcast_fusion.1
  71.6 12.9 %fusion.25 = f32[1,512,256]{1,0,2:T(1,128)S(1)} fusion(bf16[512,1,255]{0,1,2:T(2,128)(2,1)S(1)} %copy.45, bf16[1,512,510]{1,2,0:T(8,128)(2,1)S(1)} %maximum_bitcast_fusion.1), kind=kOutput, calls=%fused_computation.42 | convolution fusion | flops 66846720 | bytes 1307648 | tf_op jit(solution)/shard_map/conv_general_dilated | solution.py:47
  84.6 0.3 reduce_sum.58
  85.0 0.6 multiply_reduce_fusion.1
  85.6 0.8 fusion.30
  86.4 0.5 fusion.2
  86.9 7.4 %all_to_all.32 = bf16[2,512,256]{1,2,0:T(8,128)(2,1)S(1)} all-to-all(bf16[2,512,256]{1,2,0:T(8,128)(2,1)S(1)} %bitcast.92), channel_id=1, replica_groups=mesh['sp'=16,'tp'=2] {'tp'}, dimensions={0} | all-to-all | bytes 1048576 | tf_op jit(solution)/shard_map/all_to_all | solution.py:89
  94.4 1.0 copy.47
  (31 shorter events, 0.3 us)
Async XLA Ops:
  6.5 1.5 %copy-start = (bf16[512,512]{1,0:T(8,128)(2,1)S(1)}, bf16[512,512]{1,0:T(8,128)(2,1)}, u32[]{:S(2)}) copy-start(bf16[512,512]{1,0:T(8,128)(2,1)} %param.8) | copy-start | bytes 1572868
  6.5 15.7 %all-gather.4.cloned.1.call-start = ((), (), s32[]{:S(2)}) async-start(), calls=%async_computation.2 | async-start | bytes 3145728 | tf_op jit(solution)/shard_map/all_gather | solution.py:70
  7.3 28.3 %all-gather.6.cloned.1.call-start = ((), (), s32[]{:S(2)}) async-start(), calls=%async_computation.3 | async-start | bytes 3145728 | tf_op jit(solution)/shard_map/all_gather | solution.py:71
  9.0 5.2 %all-to-all-start = ((bf16[512,2,256]{0,2,1:T(8,128)(2,1)}), bf16[512,2,256]{0,2,1:T(8,128)(2,1)S(1)}, u32[]{:S(2)}, u32[]{:S(2)}) async-start(bf16[512,2,256]{0,2,1:T(8,128)(2,1)} %bitcast), calls=%async_computation | async-start | bytes 1048576 | tf_op jit(solution)/shard_map/all_to_all | solution.py:68
  12.5 2.2 %copy-start.2 = (f32[2,1024]{1,0:T(2,128)S(1)}, f32[2,1024]{1,0:T(2,128)}, u32[]{:S(2)}) copy-start(f32[2,1024]{1,0:T(2,128)} %param.9) | copy-start | bytes 24580
  12.5 2.3 %copy-start.1 = (bf16[2,256,255]{1,0,2:T(2,128)(2,1)S(1)}, bf16[2,256,255]{1,0,2:T(2,128)(2,1)}, u32[]{:S(2)}) copy-start(bf16[2,256,255]{1,0,2:T(2,128)(2,1)} %param.12) | copy-start | bytes 783364
  12.5 46.1 %all-gather.8.cloned.1.call-start = ((), (), s32[]{:S(2)}) async-start(), calls=%async_computation.4 | async-start | bytes 3145728 | tf_op jit(solution)/shard_map/all_gather | solution.py:73
  14.6 3.2 %copy-start.3 = (f32[2,256]{1,0:T(2,128)S(1)}, f32[2,256]{1,0:T(2,128)}, u32[]{:S(2)}) copy-start(f32[2,256]{1,0:T(2,128)} %param.13) | copy-start | bytes 6148
  14.6 5.0 %copy-start.4 = (f32[2,256]{1,0:T(2,128)S(1)}, f32[2,256]{1,0:T(2,128)}, u32[]{:S(2)}) copy-start(f32[2,256]{1,0:T(2,128)} %param.14) | copy-start | bytes 6148
  37.4 3.5 %collective-permute-start = (bf16[512,127]{0,1:T(8,128)(2,1)S(1)}, bf16[512,127]{0,1:T(8,128)(2,1)S(1)}, u32[]{:S(2)}, u32[]{:S(2)}) collective-permute-start(bf16[512,127]{0,1:T(8,128)(2,1)S(1)} %get-tuple-element.9), channel_id=1, source_target_pairs={{0,1},{1,2},{2,3},{3,4},{4,5},{5,6},{6,7},{7,8},{8,9},{9,10},{10,1... | collective-permute-start | bytes 390152 | tf_op jit(solution)/shard_map/ppermute | solution.py:21
  39.5 4.4 %collective-permute-start.1 = (bf16[512,127]{0,1:T(8,128)(2,1)S(1)}, bf16[512,127]{0,1:T(8,128)(2,1)S(1)}, u32[]{:S(2)}, u32[]{:S(2)}) collective-permute-start(bf16[512,127]{0,1:T(8,128)(2,1)S(1)} %get-tuple-element.10), channel_id=1, source_target_pairs={{1,0},{2,1},{3,2},{4,3},{5,4},{6,5},{7,6},{8,7},{9,8},{10,9},{11,1... | collective-permute-start | bytes 390152 | tf_op jit(solution)/shard_map/ppermute | solution.py:23
  58.7 2.0 %copy-start.6 = (bf16[2,512,1024]{2,1,0:T(8,128)(2,1)S(1)}, bf16[2,512,1024]{2,1,0:T(8,128)(2,1)}, u32[]{:S(2)}) copy-start(bf16[2,512,1024]{2,1,0:T(8,128)(2,1)} %all-gather.4.cloned.1.call-done) | copy-start | bytes 6291460
  60.6 1.6 %copy-start.7 = (bf16[2,512,1024]{2,1,0:T(8,128)(2,1)S(1)}, bf16[2,512,1024]{2,1,0:T(8,128)(2,1)}, u32[]{:S(2)}) copy-start(bf16[2,512,1024]{2,1,0:T(8,128)(2,1)} %all-gather.6.cloned.1.call-done) | copy-start | bytes 6291460
  62.8 7.5 %collective-permute-start.2 = (bf16[512,127]{0,1:T(8,128)(2,1)S(1)}, bf16[512,127]{0,1:T(8,128)(2,1)S(1)}, u32[]{:S(2)}, u32[]{:S(2)}) collective-permute-start(bf16[512,127]{0,1:T(8,128)(2,1)S(1)} %get-tuple-element.7), channel_id=1, source_target_pairs={{0,1},{1,2},{2,3},{3,4},{4,5},{5,6},{6,7},{7,8},{8,9},{9,10},{10,1... | collective-permute-start | bytes 390152 | tf_op jit(solution)/shard_map/ppermute | solution.py:21
  68.3 3.2 %collective-permute-start.3 = (bf16[512,127]{0,1:T(8,128)(2,1)S(1)}, bf16[512,127]{0,1:T(8,128)(2,1)S(1)}, u32[]{:S(2)}, u32[]{:S(2)}) collective-permute-start(bf16[512,127]{0,1:T(8,128)(2,1)S(1)} %get-tuple-element.8), channel_id=1, source_target_pairs={{1,0},{2,1},{3,2},{4,3},{5,4},{6,5},{7,6},{8,7},{9,8},{10,9},{11,1... | collective-permute-start | bytes 390152 | tf_op jit(solution)/shard_map/ppermute | solution.py:23
  84.6 1.8 %copy-start.5 = (bf16[2,1024,512]{2,1,0:T(8,128)(2,1)S(1)}, bf16[2,1024,512]{2,1,0:T(8,128)(2,1)}, u32[]{:S(2)}) copy-start(bf16[2,1024,512]{2,1,0:T(8,128)(2,1)} %all-gather.8.cloned.1.call-done) | copy-start | bytes 6291460
Sparse Core Ops, SparseCore 0:
  8.9 13.2 all-gather.3
  23.8 11.7 all-gather.5
  37.1 11.7 all-gather.7
where the time goes:
time: 104 us; the launch traced here: 102 us
  matrix products  32.7 us (31%)
  waiting for transfers between devices  19.1 us (18%)
  starting transfers between devices  13.9 us (13%)
  between operations  13.5 us (13%)
  blocking collectives  13.3 us (13%)
  local copies, waits for them, and re-layouts  5.15 us (5%)
  other arithmetic  4.22 us (4%)
    conv_general_dilated x2, matrix products, filter_norm(): lax.conv_general_dilated(padded[None], taps[:, None, :], (1,), [(0, 0)],...  25.8 us
    all_gather x1, waiting for transfers between devices, body(): lax.all_gather(w_gate, 'tp', axis=1, tiled=True)  11.6 us
    ppermute x2, starting transfers between devices, with_halo(): lax.ppermute(tail, axis, [(i, (i + 1) % count) for i in range(ends)])  7.59 us
    all_to_all x1, blocking collectives, body(): return lax.all_to_all(local, 'tp', split_axis=0, concat_axis=1, tiled=True)  7.44 us
    ppermute x2, waiting for transfers between devices, with_halo(): lax.ppermute(head, axis, [((i + 1) % count, i) for i in range(ends)])  4.24 us
    all_to_all x1, starting transfers between devices, body(): lax.all_to_all(stream, 'tp', split_axis=1, concat_axis=0, tiled=True)  3.49 us
    ppermute x2, starting transfers between devices, with_halo(): lax.ppermute(head, axis, [((i + 1) % count, i) for i in range(ends)])  2.76 us
    dot_general x2, matrix products, body(): jnp.dot(full_out[layer_index], activated, preferred_element_type=jnp.floa...  2.4 us
  transfers between devices with their start and end apart: 8, of which 5 were waited for; matrix products, arithmetic and copies ran while one was open for 21% of the time, Pallas kernels for 0%

commit v1 on v0

v1 whole, which is shorter than its diff:
```python
import functools

import jax
import jax.numpy as jnp
import numpy as np
from jax import lax
from jax.experimental import pallas as pl
from jax.experimental.pallas import tpu as pltpu
from jax.sharding import PartitionSpec as P

GROUP_DIM = 128
LANES = 128
RMS_EPS = 1e-06
LN_EPS = 1e-05
BF16 = jnp.bfloat16
F32 = jnp.float32


def dot(a, b):
    return jnp.dot(a, b, preferred_element_type=F32)


def sigmoid(v):
    return 0.5 + 0.5 * jnp.tanh(0.5 * v)


def fourier(rim, taps):
    size = 4 * rim
    half = size // 2
    n = np.arange(size)[:, None]
    f = np.arange(half)[None, :]
    angle = 2 * np.pi * ((n * f) % size) / size
    sine = np.sin(angle)
    sine[:, 0] = np.where(np.arange(size) % 2 == 0, 1.0, -1.0)
    forward = np.concatenate([np.cos(angle), sine], axis=1)
    scale = np.full((size, 1), 2.0 / size)
    scale[0] = scale[half] = 1.0 / size
    inverse = (forward.T * scale)[:, : 2 * rim]
    skip = rim - (taps - 1) // 2
    taps_basis = forward[skip : skip + taps]
    hi = taps_basis.astype(BF16)
    lo = (taps_basis - hi.astype(np.float64)).astype(BF16)
    return forward.astype(BF16), inverse.astype(BF16), hi, lo


def kernel(
    n_sp, layers, rim,
    stream, gain_h, wv_h, wg_h, taps_h, gg_h, gs_h, wo_h, fwd_h, inv_h, hi_h, lo_h,
    out,
    x_own, x_peer, gated, halo_l, halo_r, act, act_peer,
    gain, wvg, wo, taps, gg, gs, fwd, inv, hi, lo,
    wscaled, filt, part, spec, ggb, gsb, result,
    loads, xs_send, xs_recv, h_send, h_recv, a_send, a_recv, o_sem,
):
    sp = lax.axis_index("sp")
    tp = lax.axis_index("tp")
    peer = {"tp": 1 - tp}
    left = {"sp": jnp.maximum(sp - 1, 0)}
    right = {"sp": jnp.minimum(sp + 1, n_sp - 1)}
    has_left = sp > 0
    has_right = sp < n_sp - 1
    feats, toks = x_own.shape[1:]
    chans = act.shape[1]
    block = 2 * rim
    blocks = toks // block
    chunks = toks // rim
    own_f = pl.ds(pl.multiple_of(tp * feats, LANES), feats)
    peer_f = pl.ds(pl.multiple_of((1 - tp) * feats, LANES), feats)
    own_c = pl.ds(pl.multiple_of(tp * chans, LANES), chans)
    peer_c = pl.ds(pl.multiple_of((1 - tp) * chans, LANES), chans)

    barrier = pltpu.get_barrier_semaphore()
    pl.semaphore_signal(barrier, inc=1, device_id=peer)

    @pl.when(has_left)
    def _():
        pl.semaphore_signal(barrier, inc=1, device_id=left)

    @pl.when(has_right)
    def _():
        pl.semaphore_signal(barrier, inc=1, device_id=right)

    moves = {}

    def load(name, src, dst):
        moves[name] = pltpu.make_async_copy(src, dst, loads.at[len(moves)])
        moves[name].start()

    load("x", stream, x_own.at[0])
    load("gain", gain_h, gain)
    load("wv0", wv_h.at[0], wvg.at[0, pl.ds(0, chans)])
    load("wg0", wg_h.at[0], wvg.at[0, pl.ds(chans, chans)])
    load("taps", taps_h, taps)
    load("hi", hi_h, hi)
    load("lo", lo_h, lo)
    load("fwd", fwd_h, fwd)
    load("inv", inv_h, inv)
    load("gg", gg_h, gg)
    load("gs", gs_h, gs)
    load("wo", wo_h, wo)
    for l in range(1, layers):
        load(f"wv{l}", wv_h.at[l], wvg.at[l, pl.ds(0, chans)])
        load(f"wg{l}", wg_h.at[l], wvg.at[l, pl.ds(chans, chans)])

    def scale_weights(l):
        moves[f"wv{l}"].wait()
        moves[f"wg{l}"].wait()
        wscaled[l] = (wvg[l].astype(F32) * gain[l : l + 1, :]).astype(BF16)

    def make_filter(l):
        h = dot(taps[l], hi[...]) + dot(taps[l], lo[...])
        hc, hs = h[:, :block], h[:, block:]
        first = lax.broadcasted_iota(jnp.int32, hc.shape, 1) == 0
        filt[l, 0] = hc
        filt[l, 1] = jnp.where(first, 0.0, hs)
        filt[l, 2] = jnp.where(first, hs, hc)
        wide = (GROUP_DIM, chans)
        ggb[l] = jnp.transpose(jnp.broadcast_to(gg[l : l + 1, :], wide))
        gsb[l] = jnp.transpose(jnp.broadcast_to(gs[l : l + 1, :], wide))

    def span(c):
        return pl.ds(c * rim, rim)

    def send_x(l, c):
        move = pltpu.make_async_remote_copy(
            x_own.at[l, :, span(c)], x_peer.at[l, :, span(c)],
            xs_send.at[l, c], xs_recv.at[l, c], device_id=peer,
        )
        moves["x", l, c] = move
        move.start()

    edges = [0, chunks - 1]
    inner = list(range(1, chunks - 1))

    def pick(ref, l, cs):
        return jnp.concatenate([ref[l, :, c * rim : (c + 1) * rim] for c in cs], axis=1)

    def square_sum(x):
        wide = x.astype(F32)
        return jnp.sum(wide * wide, axis=0, keepdims=True)

    moves["x"].wait()
    moves["gain"].wait()
    scale_weights(0)
    pl.semaphore_wait(barrier, 1 + has_left.astype(jnp.int32) + has_right.astype(jnp.int32))
    for c in edges + inner:
        send_x(0, c)

    for l in range(layers):
        groups = [edges, inner]
        sums = []
        for i, cs in enumerate(groups):
            own = pick(x_own, l, cs)
            part[i] = dot(wscaled[l, :, own_f], own)
            sums.append(square_sum(own))
        if l == 0:
            for name in ("taps", "hi", "lo", "gg", "gs"):
                moves[name].wait()
            make_filter(0)
        for i, cs in enumerate(groups):
            for c in cs:
                moves["x", l, c].wait_recv()
            other = pick(x_peer, l, cs)
            total = part[i] + dot(wscaled[l, :, peer_f], other)
            mean = (sums[i] + square_sum(other)) / (2 * feats)
            total = total * lax.rsqrt(mean + RMS_EPS)
            value = total[:chans].astype(BF16).astype(F32)
            gate = total[chans:].astype(BF16).astype(F32)
            made = (value * sigmoid(gate)).astype(BF16)
            for k, c in enumerate(cs):
                gated[l, :, c * rim : (c + 1) * rim] = made[:, k * rim : (k + 1) * rim]
            if i == 0:
                to_left = pltpu.make_async_remote_copy(
                    gated.at[l, :, span(0)], halo_r.at[l],
                    h_send.at[l, 0], h_recv.at[l, 0], device_id=left,
                )
                to_right = pltpu.make_async_remote_copy(
                    gated.at[l, :, span(chunks - 1)], halo_l.at[l],
                    h_send.at[l, 1], h_recv.at[l, 1], device_id=right,
                )

                @pl.when(has_left)
                def _():
                    to_left.start()

                @pl.when(has_right)
                def _():
                    to_right.start()

        if l == 0:
            moves["fwd"].wait()
        for b in range(blocks):
            lo_c, hi_c = 2 * b - 1, 2 * b + 3
            first, last = max(lo_c, 0), min(hi_c, chunks)
            spec[b] = dot(
                gated[l, :, first * rim : last * rim],
                fwd[(first - lo_c) * rim : (last - lo_c) * rim, :],
            )
        if l + 1 < layers:
            scale_weights(l + 1)
            make_filter(l + 1)

        @pl.when(has_left)
        def _():
            to_left.wait_send()
            to_right.wait_recv()

        @pl.when(jnp.logical_not(has_left))
        def _():
            halo_l[l] = jnp.zeros(halo_l.shape[1:], BF16)

        @pl.when(has_right)
        def _():
            to_right.wait_send()
            to_left.wait_recv()

        @pl.when(jnp.logical_not(has_right))
        def _():
            halo_r[l] = jnp.zeros(halo_r.shape[1:], BF16)

        if l == 0:
            moves["inv"].wait()
        for b in range(blocks):
            s = spec[b]
            if b == 0:
                s = s + dot(halo_l[l], fwd[:rim, :])
            if b == blocks - 1:
                s = s + dot(halo_r[l], fwd[3 * rim :, :])
            re, im = s[:, :block], s[:, block:]
            y = jnp.concatenate(
                [
                    (re * filt[l, 0] + im * filt[l, 1]).astype(BF16),
                    (im * filt[l, 2] - re * filt[l, 1]).astype(BF16),
                ],
                axis=1,
            )
            filtered = dot(y, inv[...])
            for g in range(chans // GROUP_DIM):
                rows = slice(g * GROUP_DIM, (g + 1) * GROUP_DIM)
                v = filtered[rows]
                v = v - jnp.mean(v, axis=0, keepdims=True)
                v = v * lax.rsqrt(jnp.mean(v * v, axis=0, keepdims=True) + LN_EPS)
                scale = jnp.concatenate([ggb[l, rows]] * (block // GROUP_DIM), axis=1)
                shift = jnp.concatenate([gsb[l, rows]] * (block // GROUP_DIM), axis=1)
                v = v * scale + shift
                act[l, rows, b * block : (b + 1) * block] = (v * sigmoid(v)).astype(BF16)
            where = pl.ds(b * block, block)
            move = pltpu.make_async_remote_copy(
                act.at[l, :, where], act_peer.at[l, :, where],
                a_send.at[l, b], a_recv.at[l, b], device_id=peer,
            )
            moves["a", l, b] = move
            move.start()

        if l == 0:
            moves["wo"].wait()
        for b in range(blocks):
            cols = slice(b * block, (b + 1) * block)
            branch = dot(wo[l, :, own_c], act[l, :, cols])
            moves["a", l, b].wait_recv()
            branch = branch + dot(wo[l, :, peer_c], act_peer[l, :, cols])
            new = (x_own[l, :, cols].astype(F32) + branch).astype(BF16)
            if l + 1 < layers:
                x_own[l + 1, :, cols] = new
                for c in (2 * b, 2 * b + 1):
                    send_x(l + 1, c)
            else:
                result[:, cols] = new
                where = pl.ds(b * block, block)
                move = pltpu.make_async_copy(result.at[:, where], out.at[:, where], o_sem.at[b])
                moves["o", b] = move
                move.start()

    for l in range(layers):
        for c in range(chunks):
            moves["x", l, c].wait_send()
        for b in range(blocks):
            moves["a", l, b].wait_send()
    for b in range(blocks):
        moves["o", b].wait()


def body(n_sp, stream, norm_gain, w_value, w_gate, conv_taps, group_gain, group_shift, w_out):
    layers, chans, width = w_value.shape
    feats, toks = stream.shape
    n_taps = conv_taps.shape[2]
    rim = -(-(n_taps - 1) // 2 // LANES) * LANES
    block, chunks = 2 * rim, toks // rim
    blocks = toks // block
    consts = [jnp.asarray(c) for c in fourier(rim, n_taps)]
    vm = pltpu.VMEM
    dma = pltpu.SemaphoreType.DMA
    args = (stream, norm_gain, w_value, w_gate, conv_taps, group_gain, group_shift, w_out, *consts)
    return pl.pallas_call(
        functools.partial(kernel, n_sp, layers, rim),
        out_shape=jax.ShapeDtypeStruct(stream.shape, stream.dtype),
        in_specs=[pl.BlockSpec(memory_space=pl.ANY)] * len(args),
        out_specs=pl.BlockSpec(memory_space=pl.ANY),
        scratch_shapes=[
            vm((layers, feats, toks), BF16),
            vm((layers, feats, toks), BF16),
            vm((layers, chans, toks), BF16),
            vm((layers, chans, rim), BF16),
            vm((layers, chans, rim), BF16),
            vm((layers, chans, toks), BF16),
            vm((layers, chans, toks), BF16),
            vm(norm_gain.shape, F32),
            vm((layers, 2 * chans, width), BF16),
            vm(w_out.shape, BF16),
            vm(conv_taps.shape, BF16),
            vm(group_gain.shape, F32),
            vm(group_shift.shape, F32),
            *[vm(c.shape, BF16) for c in consts],
            vm((layers, 2 * chans, width), BF16),
            vm((layers, 3, chans, block), F32),
            vm((2, 2 * chans, toks // 2), F32),
            vm((blocks, chans, 2 * block), F32),
            vm((layers, chans, GROUP_DIM), F32),
            vm((layers, chans, GROUP_DIM), F32),
            vm((feats, toks), BF16),
            dma((10 + 2 * layers,)),
            dma((layers, chunks)),
            dma((layers, chunks)),
            dma((layers, 2)),
            dma((layers, 2)),
            dma((layers, blocks)),
            dma((layers, blocks)),
            dma((blocks,)),
        ],
        compiler_params=pltpu.CompilerParams(
            collective_id=0, has_side_effects=True, vmem_limit_bytes=48 * 1024 * 1024
        ),
        name="modules",
    )(*args)


def solution(mesh):
    placed = (
        P("tp", "sp"),
        P(),
        P(None, "tp", None),
        P(None, "tp", None),
        P(None, "tp", None),
        P(None, "tp"),
        P(None, "tp"),
        P(None, "tp", None),
    )
    return jax.shard_map(
        functools.partial(body, mesh.shape["sp"]),
        mesh=mesh,
        in_specs=placed,
        out_specs=P("tp", "sp"),
        check_vma=False,
    )
```

time: 104 us -> 32.4 us (0.31)
  the two profiles are of different devices: /device:TPU:0 before, /device:TPU:21 now
where the time goes in v1:
time: 32.4 us; the launch traced here: 31.9 us
  Pallas kernels  21.1 us (65%)
  local copies, waits for them, and re-layouts  10.7 us (33%)
    pallas_call x1, Pallas kernels, body(): pl.pallas_call(functools.partial(kernel, n_sp, layers, rim), out_shape=ja...  21.1 us
    unnamed x24, local copies, waits for them, and re-layouts  10.7 us

profile of v1, /device:TPU:21, one launch (start us, length us, event | category | flops | bytes accessed | tf_op | source)
XLA Modules:
  0.0 31.9 jit_solution(1746745307683670435)
XLA Ops:
  0.0 0.0 copy-start.5
  0.0 0.0 copy-start.6
  0.0 1.2 %copy.13.taps_h = bf16[2,256,255]{2,1,0:T(8,128)(2,1)S(1)} copy(bf16[2,256,255]{1,0,2:T(2,128)(2,1)} %param.16) | data formatting | bytes 522240 | tf_op args[4]
  1.2 0.0 copy-done.5
  1.2 0.0 copy-done.6
  1.2 0.0 copy-start
  1.2 1.2 %copy-done = bf16[2,256,1024]{2,1,0:T(8,128)(2,1)S(1)} copy-done((bf16[2,256,1024]{2,1,0:T(8,128)(2,1)S(1)}, bf16[2,256,1024]{2,1,0:T(8,128)(2,1)}, u32[]{:S(2)}) %copy-start) | copy-done | bytes 1048600
  2.4 0.0 copy-start.1
  2.4 1.2 %copy-done.1 = bf16[2,256,1024]{2,1,0:T(8,128)(2,1)S(1)} copy-done((bf16[2,256,1024]{2,1,0:T(8,128)(2,1)S(1)}, bf16[2,256,1024]{2,1,0:T(8,128)(2,1)}, u32[]{:S(2)}) %copy-start.1) | copy-done | bytes 1048600
  3.7 0.0 copy-start.2
  3.7 1.2 %copy-done.2 = bf16[2,512,512]{2,1,0:T(8,128)(2,1)S(1)} copy-done((bf16[2,512,512]{2,1,0:T(8,128)(2,1)S(1)}, bf16[2,512,512]{2,1,0:T(8,128)(2,1)}, u32[]{:S(2)}) %copy-start.2) | copy-done | bytes 1048600
  4.9 0.0 copy-start.3
  4.9 1.0 %copy-done.3 = bf16[512,512]{1,0:T(8,128)(2,1)S(1)} copy-done((bf16[512,512]{1,0:T(8,128)(2,1)S(1)}, bf16[512,512]{1,0:T(8,128)(2,1)}, u32[]{:S(2)}) %copy-start.3) | copy-done | bytes 524312
  5.9 0.0 copy-start.4
  5.9 1.0 %copy-done.4 = bf16[512,512]{1,0:T(8,128)(2,1)S(1)} copy-done((bf16[512,512]{1,0:T(8,128)(2,1)S(1)}, bf16[512,512]{1,0:T(8,128)(2,1)}, u32[]{:S(2)}) %copy-start.4) | copy-done | bytes 524312
  7.0 0.0 copy-start.7
  7.0 0.9 %copy-done.7 = bf16[512,256]{1,0:T(8,128)(2,1)S(1)} copy-done((bf16[512,256]{1,0:T(8,128)(2,1)S(1)}, bf16[512,256]{1,0:T(8,128)(2,1)}, u32[]{:S(2)}) %copy-start.7) | copy-done | bytes 262168
  7.9 0.0 copy-start.8
  7.9 0.7 %copy-done.8 = f32[2,1024]{1,0:T(2,128)S(1)} copy-done((f32[2,1024]{1,0:T(2,128)S(1)}, f32[2,1024]{1,0:T(2,128)}, u32[]{:S(2)}) %copy-start.8) | copy-done | bytes 8216
  8.6 0.0 copy-start.9
  8.6 0.7 %copy-done.9 = f32[2,256]{1,0:T(2,128)S(1)} copy-done((f32[2,256]{1,0:T(2,128)S(1)}, f32[2,256]{1,0:T(2,128)}, u32[]{:S(2)}) %copy-start.9) | copy-done | bytes 2072
  9.3 0.0 copy-start.10
  9.3 0.7 %copy-done.10 = f32[2,256]{1,0:T(2,128)S(1)} copy-done((f32[2,256]{1,0:T(2,128)S(1)}, f32[2,256]{1,0:T(2,128)}, u32[]{:S(2)}) %copy-start.10) | copy-done | bytes 2072
  10.0 21.1 %modules.1 = bf16[512,512]{1,0:T(8,128)(2,1)S(1)} custom-call(bf16[512,512]{1,0:T(8,128)(2,1)S(1)} %copy-done.3, f32[2,1024]{1,0:T(2,128)S(1)} %copy-done.8, bf16[2,256,1024]{2,1,0:T(8,128)(2,1)S(1)} %copy-done, bf16[2,256,1024]{2,1,0:T(8,128)(2,1)S(1)} %copy-done.1, bf16[2,256,255]{2,1,0:T(8,128)(2,1)S(1)} %copy.13.taps_h, f32[2,256]{1,0:T(2,128)S(1)} %copy-done.9, ...), custom_call_target="tpu_custom_call" | custom-call | tf_op jit(solution)/shard_map/modules/pallas_call | solution.py:294
  31.1 0.8 %copy.15 = bf16[512,512]{1,0:T(8,128)(2,1)} copy(bf16[512,512]{1,0:T(8,128)(2,1)S(1)} %modules.1) | data formatting | bytes 1048576
Async XLA Ops:
  0.0 1.2 %copy-start.5 = (bf16[255,512]{1,0:T(8,128)(2,1)S(1)}, bf16[255,512]{1,0:T(8,128)(2,1)}, u32[]{:S(2)}) copy-start(bf16[255,512]{1,0:T(8,128)(2,1)} %constant.11.clone.lo_h) | copy-start | bytes 783364
  0.0 1.2 %copy-start.6 = (bf16[255,512]{1,0:T(8,128)(2,1)S(1)}, bf16[255,512]{1,0:T(8,128)(2,1)}, u32[]{:S(2)}) copy-start(bf16[255,512]{1,0:T(8,128)(2,1)} %constant.10.clone.hi_h) | copy-start | bytes 783364
  1.2 1.2 %copy-start = (bf16[2,256,1024]{2,1,0:T(8,128)(2,1)S(1)}, bf16[2,256,1024]{2,1,0:T(8,128)(2,1)}, u32[]{:S(2)}) copy-start(bf16[2,256,1024]{2,1,0:T(8,128)(2,1)} %wv_h.1) | copy-start | bytes 3145732
  2.4 1.2 %copy-start.1 = (bf16[2,256,1024]{2,1,0:T(8,128)(2,1)S(1)}, bf16[2,256,1024]{2,1,0:T(8,128)(2,1)}, u32[]{:S(2)}) copy-start(bf16[2,256,1024]{2,1,0:T(8,128)(2,1)} %wg_h.1) | copy-start | bytes 3145732
  3.7 1.2 %copy-start.2 = (bf16[2,512,512]{2,1,0:T(8,128)(2,1)S(1)}, bf16[2,512,512]{2,1,0:T(8,128)(2,1)}, u32[]{:S(2)}) copy-start(bf16[2,512,512]{2,1,0:T(8,128)(2,1)} %wo_h.1) | copy-start | bytes 3145732
  4.9 1.0 %copy-start.3 = (bf16[512,512]{1,0:T(8,128)(2,1)S(1)}, bf16[512,512]{1,0:T(8,128)(2,1)}, u32[]{:S(2)}) copy-start(bf16[512,512]{1,0:T(8,128)(2,1)} %stream.1) | copy-start | bytes 1572868
  5.9 1.0 %copy-start.4 = (bf16[512,512]{1,0:T(8,128)(2,1)S(1)}, bf16[512,512]{1,0:T(8,128)(2,1)}, u32[]{:S(2)}) copy-start(bf16[512,512]{1,0:T(8,128)(2,1)} %constant.8.clone.fwd_h) | copy-start | bytes 1572868
  7.0 0.9 %copy-start.7 = (bf16[512,256]{1,0:T(8,128)(2,1)S(1)}, bf16[512,256]{1,0:T(8,128)(2,1)}, u32[]{:S(2)}) copy-start(bf16[512,256]{1,0:T(8,128)(2,1)} %constant.9.clone.inv_h) | copy-start | bytes 786436
  7.9 0.7 %copy-start.8 = (f32[2,1024]{1,0:T(2,128)S(1)}, f32[2,1024]{1,0:T(2,128)}, u32[]{:S(2)}) copy-start(f32[2,1024]{1,0:T(2,128)} %gain_h.1) | copy-start | bytes 24580
  8.6 0.7 %copy-start.9 = (f32[2,256]{1,0:T(2,128)S(1)}, f32[2,256]{1,0:T(2,128)}, u32[]{:S(2)}) copy-start(f32[2,256]{1,0:T(2,128)} %gg_h.1) | copy-start | bytes 6148
  9.3 0.7 %copy-start.10 = (f32[2,256]{1,0:T(2,128)S(1)}, f32[2,256]{1,0:T(2,128)}, u32[]{:S(2)}) copy-start(f32[2,256]{1,0:T(2,128)} %gs_h.1) | copy-start | bytes 6148

commit v2 on v1

--- a/solution.py
+++ b/solution.py
@@ -328,7 +328,7 @@
             dma((blocks,)),
         ],
         compiler_params=pltpu.CompilerParams(
-            collective_id=0, has_side_effects=True, vmem_limit_bytes=48 * 1024 * 1024
+            collective_id=0, has_side_effects=True, vmem_limit_bytes=67043328
         ),
         name="modules",
     )(*args)

time: 32.4 us -> 25.7 us (0.79)
  local copies, waits for them, and re-layouts: 10.7 us -> 3.69 us
  Pallas kernels: 21.1 us -> 21.8 us
    unnamed x24 -> x2, local copies, waits for them, and re-layouts: 10.7 us -> 3.69 us
    pallas_call x1, Pallas kernels: 21.1 us -> 21.8 us  [body(): pl.pallas_call(functools.partial(kernel, n_sp, layers, rim), out_shape=ja...]
where the time goes in v2:
time: 25.7 us; the launch traced here: 25.5 us
  Pallas kernels  21.8 us (85%)
  local copies, waits for them, and re-layouts  3.69 us (14%)
    pallas_call x1, Pallas kernels, body(): pl.pallas_call(functools.partial(kernel, n_sp, layers, rim), out_shape=ja...  21.8 us
    unnamed x2, local copies, waits for them, and re-layouts  3.69 us

profile of v2, /device:TPU:21, one launch (start us, length us, event | category | flops | bytes accessed | tf_op | source)
XLA Modules:
  0.0 25.5 jit_solution(13766758946149788160)
XLA Ops:
  0.0 1.8 %copy.13.taps_h = bf16[2,256,255]{2,1,0:T(8,128)(2,1)} copy(bf16[2,256,255]{1,0,2:T(2,128)(2,1)} %param.16) | data formatting | bytes 522240 | tf_op args[4]
  1.8 21.8 %modules.1 = bf16[512,512]{1,0:T(8,128)(2,1)} custom-call(bf16[512,512]{1,0:T(8,128)(2,1)} %stream.1, f32[2,1024]{1,0:T(2,128)} %gain_h.1, bf16[2,256,1024]{2,1,0:T(8,128)(2,1)} %wv_h.1, bf16[2,256,1024]{2,1,0:T(8,128)(2,1)} %wg_h.1, bf16[2,256,255]{2,1,0:T(8,128)(2,1)} %copy.13.taps_h, f32[2,256]{1,0:T(2,128)} %gg_h.1, f32[2,256]{1,0:T(2,128)} %gs_h.1, ...), custom_call_target="tpu_custom_call" | custom-call | tf_op jit(solution)/shard_map/modules/pallas_call | solution.py:294
  23.6 1.9 %copy.15 = bf16[512,512]{1,0:T(8,128)(2,1)} copy(bf16[512,512]{1,0:T(8,128)(2,1)} %modules.1) | data formatting | bytes 1048576

commit v3 on v2

v3 whole, which is shorter than its diff:
```python
import functools

import jax
import jax.numpy as jnp
import numpy as np
from jax import lax
from jax.experimental import pallas as pl
from jax.experimental.pallas import tpu as pltpu
from jax.sharding import PartitionSpec as P

GROUP_DIM = 128
LANES = 128
RMS_EPS = 1e-06
LN_EPS = 1e-05
BF16 = jnp.bfloat16
F32 = jnp.float32


def dot(a, b):
    return jnp.dot(a, b, preferred_element_type=F32)


def sigmoid(v):
    return 0.5 + 0.5 * jnp.tanh(0.5 * v)


def fourier(rim, taps):
    size = 4 * rim
    half = size // 2
    n = np.arange(size)[:, None]
    f = np.arange(half)[None, :]
    angle = 2 * np.pi * ((n * f) % size) / size
    sine = np.sin(angle)
    sine[:, 0] = np.where(np.arange(size) % 2 == 0, 1.0, -1.0)
    forward = np.concatenate([np.cos(angle), sine], axis=1)
    scale = np.full((size, 1), 2.0 / size)
    scale[0] = scale[half] = 1.0 / size
    inverse = (forward.T * scale)[:, : 2 * rim]
    skip = rim - (taps - 1) // 2
    taps_basis = forward[skip : skip + taps]
    hi = taps_basis.astype(BF16)
    lo = (taps_basis - hi.astype(np.float64)).astype(BF16)
    return forward.astype(BF16), inverse.astype(BF16), hi, lo


def kernel(
    n_sp, layers, rim,
    stream, gain_h, wv_h, wg_h, taps_h, gg_h, gs_h, wo_h, fwd_h, inv_h, hi_h, lo_h,
    out,
    x_own, x_peer, gated, halo_l, halo_r, act, act_peer,
    gain, wvg, wo, wo_peer, taps, gg, gs, fwd, inv, hi, lo,
    wscaled, filt, part, spec, ggb, gsb, result,
    loads, xs_send, xs_recv, h_send, h_recv, a_send, a_recv, w_send, w_recv, o_sem,
):
    sp = lax.axis_index("sp")
    tp = lax.axis_index("tp")
    peer = {"tp": 1 - tp}
    left = {"sp": jnp.maximum(sp - 1, 0)}
    right = {"sp": jnp.minimum(sp + 1, n_sp - 1)}
    has_left = sp > 0
    has_right = sp < n_sp - 1
    feats, toks = x_own.shape[1:]
    chans = act.shape[1]
    block = 2 * rim
    chunks = toks // rim
    last = layers - 1
    own_f = pl.ds(pl.multiple_of(tp * feats, LANES), feats)
    peer_f = pl.ds(pl.multiple_of((1 - tp) * feats, LANES), feats)
    own_c = pl.ds(pl.multiple_of(tp * chans, LANES), chans)
    peer_c = pl.ds(pl.multiple_of((1 - tp) * chans, LANES), chans)

    barrier = pltpu.get_barrier_semaphore()

    @pl.when(has_left)
    def _():
        pl.semaphore_signal(barrier, inc=1, device_id=left)

    @pl.when(has_right)
    def _():
        pl.semaphore_signal(barrier, inc=1, device_id=right)

    pl.semaphore_signal(barrier, inc=1, device_id=peer)

    moves = {}

    def load(name, src, dst):
        moves[name] = pltpu.make_async_copy(src, dst, loads.at[len(moves)])
        moves[name].start()

    load("x", stream, x_own.at[0])
    load("gain", gain_h, gain)
    load("wv0", wv_h.at[0], wvg.at[0, pl.ds(0, chans)])
    load("wg0", wg_h.at[0], wvg.at[0, pl.ds(chans, chans)])
    load("taps", taps_h, taps)
    load("hi", hi_h, hi)
    load("lo", lo_h, lo)
    load("fwd", fwd_h, fwd)
    load("inv", inv_h, inv)
    load("gg", gg_h, gg)
    load("gs", gs_h, gs)
    load("wo", wo_h, wo)
    for l in range(1, layers):
        load(f"wv{l}", wv_h.at[l], wvg.at[l, pl.ds(0, chans)])
        load(f"wg{l}", wg_h.at[l], wvg.at[l, pl.ds(chans, chans)])

    def scale_weights(l):
        moves[f"wv{l}"].wait()
        moves[f"wg{l}"].wait()
        wscaled[l] = (wvg[l].astype(F32) * gain[l : l + 1, :]).astype(BF16)

    def make_filter(l):
        mine = taps[:, l, :]
        over_taps = (((0,), (0,)), ((), ()))
        h = lax.dot_general(mine, hi[...], over_taps, preferred_element_type=F32)
        h = h + lax.dot_general(mine, lo[...], over_taps, preferred_element_type=F32)
        hc, hs = h[:, :block], h[:, block:]
        first = lax.broadcasted_iota(jnp.int32, hc.shape, 1) == 0
        filt[l, 0] = hc
        filt[l, 1] = jnp.where(first, 0.0, hs)
        filt[l, 2] = jnp.where(first, hs, hc)
        wide = (GROUP_DIM, chans)
        ggb[l] = jnp.transpose(jnp.broadcast_to(gg[l : l + 1, :], wide))
        gsb[l] = jnp.transpose(jnp.broadcast_to(gs[l : l + 1, :], wide))

    edges = [0, chunks - 1]
    inner = list(range(1, chunks - 1))
    groups = {"edges": edges, "inner": inner}

    def span(c):
        return pl.ds(c * rim, rim)

    def pick(ref, l, cs):
        return jnp.concatenate([ref[l, :, c * rim : (c + 1) * rim] for c in cs], axis=1)

    def put(ref, l, cs, value):
        for k, c in enumerate(cs):
            ref[l, :, c * rim : (c + 1) * rim] = value[:, k * rim : (k + 1) * rim]

    def remote(name, src, dst, send, recv, target):
        moves[name] = pltpu.make_async_remote_copy(src, dst, send, recv, device_id=target)
        return moves[name]

    def square_sum(x):
        wide = x.astype(F32)
        return jnp.sum(wide * wide, axis=0, keepdims=True)

    def gate(l, kind, sums, total):
        cs = groups[kind]
        other = pick(x_peer, l, cs)
        total = total + dot(wscaled[l, :, peer_f], other)
        mean = (sums + square_sum(other)) / (2 * feats)
        total = total * lax.rsqrt(mean + RMS_EPS)
        value = total[:chans].astype(BF16).astype(F32)
        gates = total[chans:].astype(BF16).astype(F32)
        put(gated, l, cs, (value * sigmoid(gates)).astype(BF16))

    def project(l, kind):
        own = pick(x_own, l, groups[kind])
        gate(l, kind, square_sum(own), dot(wscaled[l, :, own_f], own))

    def send_halo(l):
        to_left = remote(("l", l), gated.at[l, :, span(0)], halo_r.at[l],
                         h_send.at[l, 0], h_recv.at[l, 0], left)
        to_right = remote(("r", l), gated.at[l, :, span(chunks - 1)], halo_l.at[l],
                          h_send.at[l, 1], h_recv.at[l, 1], right)

        @pl.when(has_right)
        def _():
            to_right.start()

        @pl.when(has_left)
        def _():
            to_left.start()

    def wait_halo(l, has, out_name, in_name, halo):
        @pl.when(has)
        def _():
            moves[out_name, l].wait_send()
            moves[in_name, l].wait_recv()

        @pl.when(jnp.logical_not(has))
        def _():
            halo[l] = jnp.zeros(halo.shape[1:], BF16)

    def activate(l, s, start, width):
        re, im = s[:, :block], s[:, block:]
        y = jnp.concatenate(
            [
                (re * filt[l, 0] + im * filt[l, 1]).astype(BF16),
                (im * filt[l, 2] - re * filt[l, 1]).astype(BF16),
            ],
            axis=1,
        )
        filtered = dot(y, inv[:, :width])
        for g in range(chans // GROUP_DIM):
            rows = slice(g * GROUP_DIM, (g + 1) * GROUP_DIM)
            v = filtered[rows]
            v = v - jnp.mean(v, axis=0, keepdims=True)
            v = v * lax.rsqrt(jnp.mean(v * v, axis=0, keepdims=True) + LN_EPS)
            scale = jnp.concatenate([ggb[l, rows]] * (width // GROUP_DIM), axis=1)
            shift = jnp.concatenate([gsb[l, rows]] * (width // GROUP_DIM), axis=1)
            v = v * scale + shift
            act[l, rows, start : start + width] = (v * sigmoid(v)).astype(BF16)
        where = pl.ds(start, width)
        k = {0: 0, rim: 1, toks - rim: 2}[start]
        remote(("a", l, k), act.at[l, :, where], act_peer.at[l, :, where],
               a_send.at[l, k], a_recv.at[l, k], peer).start()

    def project_out(l, kind, arrivals):
        cs = groups[kind]
        mine = pick(act, l, cs)
        branch = dot(wo[l, :, own_c], mine)
        if l < last:
            there = dot(wo_peer[l, :, own_c], mine)
        for k in arrivals:
            moves["a", l, k].wait_recv()
        other = pick(act_peer, l, cs)
        branch = branch + dot(wo[l, :, peer_c], other)
        new = (pick(x_own, l, cs).astype(F32) + branch).astype(BF16)
        if l < last:
            there = there + dot(wo_peer[l, :, peer_c], other)
            put(x_own, l + 1, cs, new)
            put(x_peer, l + 1, cs, (pick(x_peer, l, cs).astype(F32) + there).astype(BF16))
        else:
            for k, c in enumerate(cs):
                result[:, c * rim : (c + 1) * rim] = new[:, k * rim : (k + 1) * rim]
                move = pltpu.make_async_copy(
                    result.at[:, span(c)], out.at[:, span(c)], o_sem.at[c]
                )
                moves["o", c] = move
                move.start()

    moves["x"].wait()
    moves["gain"].wait()
    scale_weights(0)
    pl.semaphore_wait(barrier, 1 + has_left.astype(jnp.int32) + has_right.astype(jnp.int32))
    for c in edges + inner:
        remote(("x", c), x_own.at[0, :, span(c)], x_peer.at[0, :, span(c)],
               xs_send.at[c], xs_recv.at[c], peer).start()
    for l in range(last):
        remote(("w", l), wo_h.at[l], wo_peer.at[l], w_send.at[l], w_recv.at[l], peer).start()

    sums = {}
    for i, kind in enumerate(groups):
        own = pick(x_own, 0, groups[kind])
        part[i] = dot(wscaled[0, :, own_f], own)
        sums[kind] = square_sum(own)
    for name in ("taps", "hi", "lo", "gg", "gs"):
        moves[name].wait()
    make_filter(0)
    for i, kind in enumerate(groups):
        for c in groups[kind]:
            moves["x", c].wait_recv()
        gate(0, kind, sums[kind], part[i])
        if kind == "edges":
            send_halo(0)

    for l in range(layers):
        if l == 0:
            moves["fwd"].wait()
            moves["inv"].wait()
        activate(l, dot(gated[l], fwd[...]), rim, block)
        spec[0] = dot(gated[l, :, :block], fwd[rim : rim + block, :])
        spec[1] = dot(gated[l, :, toks - block :], fwd[:block, :])
        if l == 0:
            moves["wo"].wait()
        if l < last:
            scale_weights(l + 1)
            make_filter(l + 1)
            moves["w", l].wait_recv()
        project_out(l, "inner", (1,))
        if l < last:
            project(l + 1, "inner")
        wait_halo(l, has_left, "l", "r", halo_l)
        activate(l, spec[0] + dot(halo_l[l], fwd[:rim, :]), 0, rim)
        wait_halo(l, has_right, "r", "l", halo_r)
        activate(l, spec[1] + dot(halo_r[l], fwd[block : block + rim, :]), toks - rim, rim)
        project_out(l, "edges", (0, 2))
        if l < last:
            project(l + 1, "edges")
            send_halo(l + 1)

    for c in range(chunks):
        moves["x", c].wait_send()
        moves["o", c].wait()
    for l in range(last):
        moves["w", l].wait_send()
    for l in range(layers):
        for k in range(3):
            moves["a", l, k].wait_send()


def body(n_sp, stream, norm_gain, w_value, w_gate, conv_taps, group_gain, group_shift, w_out):
    layers, chans, width = w_value.shape
    feats, toks = stream.shape
    n_taps = conv_taps.shape[2]
    rim = -(-(n_taps - 1) // 2 // LANES) * LANES
    block, chunks = 2 * rim, toks // rim
    consts = [jnp.asarray(c) for c in fourier(rim, n_taps)]
    vm = pltpu.VMEM
    dma = pltpu.SemaphoreType.DMA
    by_tap = jnp.transpose(conv_taps, (2, 0, 1))
    args = (stream, norm_gain, w_value, w_gate, by_tap, group_gain, group_shift, w_out, *consts)
    return pl.pallas_call(
        functools.partial(kernel, n_sp, layers, rim),
        out_shape=jax.ShapeDtypeStruct(stream.shape, stream.dtype),
        in_specs=[pl.BlockSpec(memory_space=pl.ANY)] * len(args),
        out_specs=pl.BlockSpec(memory_space=pl.ANY),
        scratch_shapes=[
            vm((layers, feats, toks), BF16),
            vm((layers, feats, toks), BF16),
            vm((layers, chans, toks), BF16),
            vm((layers, chans, rim), BF16),
            vm((layers, chans, rim), BF16),
            vm((layers, chans, toks), BF16),
            vm((layers, chans, toks), BF16),
            vm(norm_gain.shape, F32),
            vm((layers, 2 * chans, width), BF16),
            vm(w_out.shape, BF16),
            vm((max(layers - 1, 1), *w_out.shape[1:]), BF16),
            vm(by_tap.shape, BF16),
            vm(group_gain.shape, F32),
            vm(group_shift.shape, F32),
            *[vm(c.shape, BF16) for c in consts],
            vm((layers, 2 * chans, width), BF16),
            vm((layers, 3, chans, block), F32),
            vm((2, 2 * chans, toks // 2), F32),
            vm((2, chans, 2 * block), F32),
            vm((layers, chans, GROUP_DIM), F32),
            vm((layers, chans, GROUP_DIM), F32),
            vm((feats, toks), BF16),
            dma((10 + 2 * layers,)),
            dma((chunks,)),
            dma((chunks,)),
            dma((layers, 2)),
            dma((layers, 2)),
            dma((layers, 3)),
            dma((layers, 3)),
            dma((layers,)),
            dma((layers,)),
            dma((chunks,)),
        ],
        compiler_params=pltpu.CompilerParams(
            collective_id=0, has_side_effects=True, vmem_limit_bytes=67043328
        ),
        name="modules",
    )(*args)


def solution(mesh):
    placed = (
        P("tp", "sp"),
        P(),
        P(None, "tp", None),
        P(None, "tp", None),
        P(None, "tp", None),
        P(None, "tp"),
        P(None, "tp"),
        P(None, "tp", None),
    )
    return jax.shard_map(
        functools.partial(body, mesh.shape["sp"]),
        mesh=mesh,
        in_specs=placed,
        out_specs=P("tp", "sp"),
        check_vma=False,
    )
```

time: 25.7 us -> 23.1 us (0.90)
  the two profiles are of different devices: /device:TPU:21 before, /device:TPU:0 now
where the time goes in v3:
time: 23.1 us; the launch traced here: 22.9 us
  Pallas kernels  21.1 us (91%)
  local copies, waits for them, and re-layouts  1.87 us (8%)
    pallas_call x1, Pallas kernels, body(): pl.pallas_call(functools.partial(kernel, n_sp, layers, rim), out_shape=ja...  21.1 us
    unnamed x1, local copies, waits for them, and re-layouts  1.87 us

profile of v3, /device:TPU:0, one launch (start us, length us, event | category | flops | bytes accessed | tf_op | source)
XLA Modules:
  0.0 22.9 jit_solution(3407228390062532790)
XLA Ops:
  0.0 21.1 %modules.1 = bf16[512,512]{1,0:T(8,128)(2,1)} custom-call(bf16[512,512]{1,0:T(8,128)(2,1)} %stream.1, f32[2,1024]{1,0:T(2,128)} %gain_h.1, bf16[2,256,1024]{2,1,0:T(8,128)(2,1)} %wv_h.1, bf16[2,256,1024]{2,1,0:T(8,128)(2,1)} %wg_h.1, bf16[255,2,256]{2,1,0:T(2,128)(2,1)} %bitcast.1, f32[2,256]{1,0:T(2,128)} %gg_h.1, f32[2,256]{1,0:T(2,128)} %gs_h.1, ...), custom_call_target="tpu_custom_call" | custom-call | tf_op jit(solution)/shard_map/modules/pallas_call | solution.py:304
  21.1 1.9 %copy.14 = bf16[512,512]{1,0:T(8,128)(2,1)} copy(bf16[512,512]{1,0:T(8,128)(2,1)} %modules.1) | data formatting | bytes 1048576

commit v4 on v3

--- a/solution.py
+++ b/solution.py
@@ -49,8 +49,8 @@
     out,
     x_own, x_peer, gated, halo_l, halo_r, act, act_peer,
     gain, wvg, wo, wo_peer, taps, gg, gs, fwd, inv, hi, lo,
-    wscaled, filt, part, spec, ggb, gsb, result,
-    loads, xs_send, xs_recv, h_send, h_recv, a_send, a_recv, w_send, w_recv, o_sem,
+    wscaled, filt, part, spec, ggb, gsb,
+    loads, xs_send, xs_recv, h_send, h_recv, a_send, a_recv, w_send, w_recv,
 ):
     sp = lax.axis_index("sp")
     tp = lax.axis_index("tp")
@@ -223,12 +223,7 @@
             put(x_peer, l + 1, cs, (pick(x_peer, l, cs).astype(F32) + there).astype(BF16))
         else:
             for k, c in enumerate(cs):
-                result[:, c * rim : (c + 1) * rim] = new[:, k * rim : (k + 1) * rim]
-                move = pltpu.make_async_copy(
-                    result.at[:, span(c)], out.at[:, span(c)], o_sem.at[c]
-                )
-                moves["o", c] = move
-                move.start()
+                out[:, c * rim : (c + 1) * rim] = new[:, k * rim : (k + 1) * rim]
 
     moves["x"].wait()
     moves["gain"].wait()
@@ -245,15 +240,15 @@
         own = pick(x_own, 0, groups[kind])
         part[i] = dot(wscaled[0, :, own_f], own)
         sums[kind] = square_sum(own)
-    for name in ("taps", "hi", "lo", "gg", "gs"):
-        moves[name].wait()
-    make_filter(0)
     for i, kind in enumerate(groups):
         for c in groups[kind]:
             moves["x", c].wait_recv()
         gate(0, kind, sums[kind], part[i])
         if kind == "edges":
             send_halo(0)
+    for name in ("taps", "hi", "lo", "gg", "gs"):
+        moves[name].wait()
+    make_filter(0)
 
     for l in range(layers):
         if l == 0:
@@ -282,7 +277,6 @@
 
     for c in range(chunks):
         moves["x", c].wait_send()
-        moves["o", c].wait()
     for l in range(last):
         moves["w", l].wait_send()
     for l in range(layers):
@@ -303,9 +297,9 @@
     args = (stream, norm_gain, w_value, w_gate, by_tap, group_gain, group_shift, w_out, *consts)
     return pl.pallas_call(
         functools.partial(kernel, n_sp, layers, rim),
-        out_shape=jax.ShapeDtypeStruct(stream.shape, stream.dtype),
+        out_shape=pltpu.VMEM(stream.shape, stream.dtype),
         in_specs=[pl.BlockSpec(memory_space=pl.ANY)] * len(args),
-        out_specs=pl.BlockSpec(memory_space=pl.ANY),
+        out_specs=pl.BlockSpec(memory_space=pltpu.VMEM),
         scratch_shapes=[
             vm((layers, feats, toks), BF16),
             vm((layers, feats, toks), BF16),
@@ -328,7 +322,6 @@
             vm((2, chans, 2 * block), F32),
             vm((layers, chans, GROUP_DIM), F32),
             vm((layers, chans, GROUP_DIM), F32),
-            vm((feats, toks), BF16),
             dma((10 + 2 * layers,)),
             dma((chunks,)),
             dma((chunks,)),
@@ -338,10 +331,9 @@
             dma((layers, 3)),
             dma((layers,)),
             dma((layers,)),
-            dma((chunks,)),
         ],
         compiler_params=pltpu.CompilerParams(
-            collective_id=0, has_side_effects=True, vmem_limit_bytes=67043328
+            collective_id=0, has_side_effects=True, vmem_limit_bytes=66000000
         ),
         name="modules",
     )(*args)

time: 23.1 us -> 21.2 us (0.918)
  local copies, waits for them, and re-layouts: 1.87 us -> 0.8 us
  Pallas kernels: 21.1 us -> 20.1 us
    unnamed x1, local copies, waits for them, and re-layouts: 1.87 us -> 0.8 us
    pallas_call x1, Pallas kernels: 21.1 us -> 20.1 us  [body(): pl.pallas_call(functools.partial(kernel, n_sp, layers, rim), out_shape=pl...]
where the time goes in v4:
time: 21.2 us; the launch traced here: 20.9 us
  Pallas kernels  20.1 us (95%)
  local copies, waits for them, and re-layouts  0.8 us (4%)
    pallas_call x1, Pallas kernels, body(): pl.pallas_call(functools.partial(kernel, n_sp, layers, rim), out_shape=pl...  20.1 us
    unnamed x1, local copies, waits for them, and re-layouts  0.8 us

profile of v4, /device:TPU:0, one launch (start us, length us, event | category | flops | bytes accessed | tf_op | source)
XLA Modules:
  0.0 20.9 jit_solution(10317669298287047393)
XLA Ops:
  0.0 20.1 %modules.1 = bf16[512,512]{1,0:T(8,128)(2,1)S(1)} custom-call(bf16[512,512]{1,0:T(8,128)(2,1)} %stream.1, f32[2,1024]{1,0:T(2,128)} %gain_h.1, bf16[2,256,1024]{2,1,0:T(8,128)(2,1)} %wv_h.1, bf16[2,256,1024]{2,1,0:T(8,128)(2,1)} %wg_h.1, bf16[255,2,256]{2,1,0:T(2,128)(2,1)} %bitcast.1, f32[2,256]{1,0:T(2,128)} %gg_h.1, f32[2,256]{1,0:T(2,128)} %gs_h.1, ...), custom_call_target="tpu_custom_call" | custom-call | tf_op jit(solution)/shard_map/modules/pallas_call | solution.py:298
  20.1 0.8 %copy.14 = bf16[512,512]{1,0:T(8,128)(2,1)} copy(bf16[512,512]{1,0:T(8,128)(2,1)S(1)} %modules.1) | data formatting | bytes 1048576
